TPU v7x, 32 devices: a whole 2x2x4 slice. The times are simulated.
32 devices in a mesh: ep: 8 (over z, x), tp: 4 (over y, core).
Axes of the slice: x: 2, y: 2, z: 4, core: 2. Of those that a mesh axis runs over, the one named last changes fastest.
Arguments:
- projected_queries: bfloat16 [2048, 2048], P('ep', 'tp'), may hold values from -245 to 245, as said below
- key_proj: bfloat16 [2048, 512], P('ep', 'tp'), may hold values from -6.2 to 6.2
- projected_values: bfloat16 [2048, 512], P('ep', 'tp'), may hold values from -24 to 24
- head_sink_logits: float32 [32], P('tp'), may hold values from 1 to 6
- out_weight: bfloat16 [2048, 4096], P('tp'), may hold values from -0.125 to 0.125
- expert_input: bfloat16 [1024, 4096], P('ep'), may hold values from -6 to 6
- norm_gain: float32 [4096], replicated, may hold values from 0.1 to 1.9
- routing: int32 [1024, 4], P('ep'), may hold values from 0 to 7, all different within a row; in each aligned block of 128 rows (0 to 127, 128 to 255, ...) at most 96 rows name the same one
- route_weight: float32 [1024, 4], P('ep'), may hold values from 0.1 to 1
- gate_weight: bfloat16 [8, 4096, 1024], P('ep', None, 'tp'), may hold values from -0.27929688 to 0.27929688
- up_weight: bfloat16 [8, 4096, 1024], P('ep', None, 'tp'), may hold values from -0.27929688 to 0.27929688
- down_weight: bfloat16 [8, 1024, 4096], P('ep', 'tp'), may hold values from -0.046875 to 0.046875
Outputs:
- mixer_output: bfloat16 [2048, 4096], P(('ep', 'tp'))
- expert_output: bfloat16 [1024, 4096], P('ep', 'tp')
Inputs may be any that keep to these rules, and one draw needn't show every extreme that they name: `projected_queries`: in the hidden draw some queries nearly equal a large multiple of a nearby key. `routing`: each row names 4 different experts; among the rows of one device (aligned blocks of 128 rows) no expert is named more than 96 times, a bound that some block reaches.
All inputs are finite; a program needn't handle non-finite values.
Results may differ from a plain program's by a relative error of at most 0.014.
Values may be sent and summed in bfloat16 or wider, within the bound.
A program may use at most 128 MiB of HBM per device.

v0:
```python
import jax
import jax.numpy as jnp
from jax import lax
from jax.sharding import PartitionSpec as P

D = 4096
HEAD_SIZE = 64
WINDOW_KEYS = 128
TOPK = 4
EPS = 1e-06
CLAMP = 7.0
SLOPE = 1.702


def passed_along(block, axis, distance):
    devices = range(lax.axis_size(axis))
    route = [(i - distance, i) for i in devices if i - distance in devices]
    return lax.ppermute(block, axis, route)


def shards(
    projected_queries,
    key_proj,
    projected_values,
    head_sink_logits,
    out_weight,
    expert_input,
    norm_gain,
    routing,
    route_weight,
    gate_weight,
    up_weight,
    down_weight,
):
    query_rows = projected_queries.shape[0]
    kv_heads = key_proj.shape[1] // HEAD_SIZE
    heads_per_group = projected_queries.shape[1] // HEAD_SIZE // kv_heads
    count_of_blocks = query_rows // WINDOW_KEYS
    prior_key, prior_value = passed_along(
        (key_proj[query_rows - WINDOW_KEYS :], projected_values[query_rows - WINDOW_KEYS :]),
        "ep",
        1,
    )
    key_all = jnp.concatenate([prior_key, key_proj], axis=0)
    value_all = jnp.concatenate([prior_value, projected_values], axis=0)
    window_keys = jnp.concatenate(
        [
            key_all[:-WINDOW_KEYS].reshape(count_of_blocks, WINDOW_KEYS, kv_heads, HEAD_SIZE),
            key_all[WINDOW_KEYS:].reshape(count_of_blocks, WINDOW_KEYS, kv_heads, HEAD_SIZE),
        ],
        axis=1,
    )
    window_values = jnp.concatenate(
        [
            value_all[:-WINDOW_KEYS].reshape(count_of_blocks, WINDOW_KEYS, kv_heads, HEAD_SIZE),
            value_all[WINDOW_KEYS:].reshape(count_of_blocks, WINDOW_KEYS, kv_heads, HEAD_SIZE),
        ],
        axis=1,
    )
    query_blocks = projected_queries.reshape(
        count_of_blocks, WINDOW_KEYS, kv_heads, heads_per_group, HEAD_SIZE
    )
    scores = jnp.einsum(
        "nqhgd,nshd->nhgqs", query_blocks, window_keys, preferred_element_type=jnp.float32
    ) * HEAD_SIZE ** (-0.5)
    offset = lax.axis_index("ep") * query_rows
    block_ids = jnp.arange(count_of_blocks)[:, None, None] * WINDOW_KEYS + offset
    query_pos = block_ids + jnp.arange(WINDOW_KEYS)[None, :, None]
    key_pos = block_ids - WINDOW_KEYS + jnp.arange(2 * WINDOW_KEYS)[None, None, :]
    permitted_mask = (key_pos <= query_pos) & (query_pos - key_pos < WINDOW_KEYS) & (key_pos >= 0)
    scores = jnp.where(permitted_mask[:, None, None, :, :], scores, -jnp.inf)
    sink_col = head_sink_logits.reshape(kv_heads, heads_per_group)[None, :, :, None, None]
    highest = jnp.maximum(jnp.max(scores, axis=-1, keepdims=True), sink_col)
    numerator = jnp.exp(scores - highest)
    denominator = jnp.sum(numerator, axis=-1, keepdims=True) + jnp.exp(sink_col - highest)
    weights = (numerator / denominator).astype(jnp.bfloat16)
    attended = jnp.einsum(
        "nhgqs,nshd->nqhgd", weights, window_values, preferred_element_type=jnp.float32
    )
    attended = attended.astype(jnp.bfloat16).reshape(
        query_rows, kv_heads * heads_per_group * HEAD_SIZE
    )
    mixer_output = lax.psum_scatter(
        jnp.dot(attended, out_weight, preferred_element_type=jnp.float32).astype(jnp.bfloat16),
        "tp",
        scatter_dimension=0,
        tiled=True,
    )
    token_rows = expert_input.shape[0]
    experts = lax.axis_size("ep")
    capacity = max(3 * token_rows * TOPK // (2 * experts), 2)
    col_share = D // lax.axis_size("tp")
    widened = expert_input.astype(jnp.float32)
    normed = (
        widened
        * lax.rsqrt(jnp.mean(widened * widened, axis=-1, keepdims=True) + EPS)
        * norm_gain[None, :]
    ).astype(jnp.bfloat16)
    flat_ids = routing.reshape(-1)
    onehot = (flat_ids[:, None] == jnp.arange(experts, dtype=jnp.int32)[None, :]).astype(jnp.int32)
    rank_in = jnp.cumsum(onehot, axis=0) - 1
    target = flat_ids * capacity + jnp.sum(rank_in * onehot, axis=1)
    tok_ids = jnp.arange(token_rows * TOPK) // TOPK
    slot_tok = jnp.full((experts * capacity,), token_rows, jnp.int32).at[target].set(tok_ids)
    gate_one = gate_weight[0]
    up_one = up_weight[0]
    own_cols = lax.dynamic_slice_in_dim(normed, lax.axis_index("tp") * col_share, col_share, 1)
    extended = jnp.concatenate([own_cols, jnp.zeros((1, col_share), jnp.bfloat16)], axis=0)
    outgoing = jnp.take(extended, slot_tok, axis=0).reshape(experts, capacity, col_share)
    arrived = lax.all_to_all(outgoing, "ep", split_axis=0, concat_axis=0, tiled=True).reshape(
        experts * capacity, col_share
    )
    portion = lax.all_gather(arrived, "tp", axis=1, tiled=True)
    gate_pre = jnp.dot(portion, gate_one, preferred_element_type=jnp.float32)
    up_pre = jnp.dot(portion, up_one, preferred_element_type=jnp.float32)
    gate_cut = jnp.minimum(gate_pre, CLAMP)
    activated = (
        (jnp.clip(up_pre, -CLAMP, CLAMP) + 1.0) * gate_cut * jax.nn.sigmoid(SLOPE * gate_cut)
    ).astype(jnp.bfloat16)
    partial_value = jnp.dot(activated, down_weight[0], preferred_element_type=jnp.float32)
    expert_result = lax.psum_scatter(
        partial_value.astype(jnp.bfloat16), "tp", scatter_dimension=1, tiled=True
    )
    returned = lax.all_to_all(
        expert_result.reshape(experts, capacity, col_share),
        "ep",
        split_axis=0,
        concat_axis=0,
        tiled=True,
    )
    picked = jnp.take(returned.reshape(experts * capacity, col_share), target, axis=0)
    picked = picked.astype(jnp.float32).reshape(token_rows, TOPK, col_share)
    expert_output = jnp.sum(picked * route_weight[:, :, None], axis=1).astype(jnp.bfloat16)
    return (mixer_output, expert_output)


def solution(mesh):
    placed = (
        P("ep", "tp"),
        P("ep", "tp"),
        P("ep", "tp"),
        P("tp"),
        P("tp", None),
        P("ep", None),
        P(),
        P("ep", None),
        P("ep", None),
        P("ep", None, "tp"),
        P("ep", None, "tp"),
        P("ep", "tp", None),
    )
    return jax.shard_map(
        shards,
        mesh=mesh,
        in_specs=placed,
        out_specs=(P(("ep", "tp"), None), P("ep", "tp")),
        check_vma=False,
    )
```

profile of v0, /device:TPU:0, one launch (start us, length us, event | category | flops | bytes accessed | tf_op | source)
XLA Modules:
  0.0 246.2 jit_solution(7340603953749888694)
XLA Ops:
  7.2 2.9 %convert_element_type.41 = f32[128,4096]{1,0:T(8,128)} convert(bf16[128,4096]{1,0:T(8,128)(2,1)} %param.17) | non-fusion elementwise | flops 524288 | bytes 3145728 | tf_op jit(solution)/shard_map/convert_element_type | solution.py:93
  10.2 0.3 multiply_reduce_fusion.1
  10.8 1.1 reduce-window.6
  12.0 0.2 slice_reduce_fusion
  12.6 2.4 scatter_custom_fusion
  15.2 0.7 dynamic-slice
  15.9 1.1 fusion.33
  17.1 3.6 %gather_fusion = bf16[768,1024]{1,0:T(8,128)(2,1)} fusion(bf16[129,1024]{1,0:T(8,128)(2,1)S(1)} %concatenate.19, s32[1024]{0:T(1024)S(1)} %pad_clamp_fusion.1), kind=kCustom, calls=%fused_computation | custom fusion | bytes 3148800 | tf_op jit(solution)/shard_map/jit(_take)/gather | solution.py:109
  20.6 1.6 broadcast_select_fusion
  22.3 44.2 %all_to_all.10 = bf16[8,96,1024]{2,1,0:T(8,128)(2,1)} all-to-all(bf16[8,96,1024]{2,1,0:T(8,128)(2,1)S(1)} %broadcast_select_fusion), channel_id=1, replica_groups=mesh['ep'=8,'tp'=4] {'ep'}, dimensions={0} | all-to-all | bytes 3145728 | tf_op jit(solution)/shard_map/all_to_all | solution.py:110
  66.5 45.5 %all-gather.2.cloned.1.call-done = bf16[768,4096]{1,0:T(8,128)(2,1)} async-done(((bf16[768,1024]{1,0:T(8,128)(2,1)}), bf16[768,4096]{1,0:T(8,128)(2,1)}) %all-gather.2.cloned.1.call-update) | async-done | bytes 6291472 | tf_op jit(solution)/shard_map/all_gather | solution.py:113
  112.0 5.2 %fusion.9 = f32[768,256]{1,0:T(8,128)S(1)} fusion(bf16[768,4096]{1,0:T(8,128)(2,1)} %all-gather.2.cloned.1.call-done, bf16[1,4096,256]{2,1,0:T(8,128)(2,1)} %param.21), kind=kOutput, calls=%fused_computation.18 | convolution fusion | flops 1610809344 | bytes 9175040 | tf_op jit(solution)/shard_map/dot_general | solution.py:114
  117.2 12.7 %convolution_convert_fusion = bf16[768,4096]{1,0:T(8,128)(2,1)} fusion(bf16[1,256,4096]{2,1,0:T(8,128)(2,1)S(1)} %copy-done, f32[768,256]{1,0:T(8,128)S(1)} %fusion.9, bf16[768,4096]{1,0:T(8,128)(2,1)} %all-gather.2.cloned.1.call-done, bf16[1,4096,256]{2,1,0:T(8,128)(2,1)} %param.22), kind=kOutput, calls=%fused_computation.3 | convolution fusion | flops 3226140672 | bytes 17563648 | tf_op jit(solution)/shard_map/dot_general | solution.py:120
  130.0 0.8 copy-done.3
  130.8 3.4 %collective-permute-start.1 = (bf16[128,128]{1,0:T(8,128)(2,1)S(1)}, bf16[128,128]{1,0:T(8,128)(2,1)S(1)}, u32[]{:S(2)}, u32[]{:S(2)}) collective-permute-start(bf16[128,128]{1,0:T(8,128)(2,1)S(1)} %slice.20), channel_id=1, source_target_pairs={{0,4},{4,8},{8,12},{12,16},{16,20},{20,24},{24,28},{1,5},{5,9},{9,... | collective-permute-start | bytes 98312 | tf_op jit(solution)/shard_map/ppermute | solution.py:18
  134.2 3.6 %collective-permute-start = (bf16[128,128]{1,0:T(8,128)(2,1)S(1)}, bf16[128,128]{1,0:T(8,128)(2,1)S(1)}, u32[]{:S(2)}, u32[]{:S(2)}) collective-permute-start(bf16[128,128]{1,0:T(8,128)(2,1)S(1)} %slice.18), channel_id=1, source_target_pairs={{0,4},{4,8},{8,12},{12,16},{16,20},{20,24},{24,28},{1,5},{5,9},{9,... | collective-permute-start | bytes 98312 | tf_op jit(solution)/shard_map/ppermute | solution.py:18
  138.0 0.2 fusion.42
  138.4 0.3 reshape.255
  139.5 0.5 fusion.60
  140.1 0.3 fusion.5
  140.5 0.5 fusion.26
  141.0 0.3 copy.45
  141.2 1.7 copy-done.2
  143.0 2.7 %convolution_convert_fusion.1 = bf16[256,4096]{1,0:T(8,128)(2,1)} fusion(bf16[512,4096]{1,0:T(8,128)(2,1)S(1)} %copy-done.2, bf16[64,8,2,128]{3,2,1,0:T(2,128)(2,1)S(1)} %bitcast.64), kind=kOutput, calls=%fused_computation.4 | convolution fusion | flops 1074790400 | bytes 6553600 | tf_op jit(solution)/shard_map/dot_general | solution.py:84
  145.7 42.3 %reduce-scatter.5.cloned.1.call-done = bf16[768,1024]{1,0:T(8,128)(2,1)} async-done(((bf16[768,4096]{1,0:T(8,128)(2,1)}), bf16[768,1024]{1,0:T(8,128)(2,1)}) %reduce-scatter.5.cloned.1.call-update) | async-done | bytes 1572880 | tf_op jit(solution)/shard_map/reduce_scatter | solution.py:121
  188.0 5.5 %all-to-all-start.1 = ((bf16[8,96,1024]{2,1,0:T(8,128)(2,1)}), bf16[8,96,1024]{2,1,0:T(8,128)(2,1)}, u32[]{:S(2)}, u32[]{:S(2)}) async-start(bf16[8,96,1024]{2,1,0:T(8,128)(2,1)} %bitcast.63), calls=%async_computation.3 | async-start | bytes 3145728 | tf_op jit(solution)/shard_map/all_to_all | solution.py:124
  193.7 0.1 copy.49
  193.9 0.1 copy.51
  194.0 36.5 %all-to-all-done.1 = bf16[8,96,1024]{2,1,0:T(8,128)(2,1)} async-done(((bf16[8,96,1024]{2,1,0:T(8,128)(2,1)}), bf16[8,96,1024]{2,1,0:T(8,128)(2,1)}, u32[]{:S(2)}, u32[]{:S(2)}) %all-to-all-start.1) | async-done | bytes 1572896 | tf_op jit(solution)/shard_map/all_to_all | solution.py:124
  230.4 4.3 %gather_fusion.1 = bf16[512,1024]{1,0:T(8,128)(2,1)S(1)} fusion(bf16[768,1024]{1,0:T(8,128)(2,1)} %bitcast.16, s32[1024]{0:T(1024)S(1)} %pad_clamp_fusion), kind=kCustom, calls=%fused_computation.1 | custom fusion | bytes 2099200 | tf_op jit(solution)/shard_map/jit(_take)/gather | solution.py:131
  234.8 1.2 gather.15
  236.0 3.6 %multiply_reduce_fusion = bf16[128,1024]{1,0:T(8,128)(2,1)} fusion(f32[128,4]{1,0:T(8,128)S(1)} %copy.51, bf16[128,4,1024]{2,1,0:T(4,128)(2,1)} %gather.15, pred[128,4]{1,0:T(8,128)(4,1)S(1)} %copy.49), kind=kLoop, calls=%fused_computation.11 | loop fusion | flops 1966080 | bytes 1313280 | tf_op jit(solution)/shard_map/reduce_sum | solution.py:133
  (66 shorter events, 2.5 us)
Async XLA Ops:
  7.2 110.1 %copy-start = (bf16[1,256,4096]{2,1,0:T(8,128)(2,1)S(1)}, bf16[1,256,4096]{2,1,0:T(8,128)(2,1)}, u32[]{:S(2)}) copy-start(bf16[1,256,4096]{2,1,0:T(8,128)(2,1)} %param.23) | copy-start | bytes 6291460
  7.2 3.0 %copy-start.1 = (bf16[128,4096]{1,0:T(8,128)(2,1)S(1)}, bf16[128,4096]{1,0:T(8,128)(2,1)}, u32[]{:S(2)}) copy-start(bf16[128,4096]{1,0:T(8,128)(2,1)} %param.17) | copy-start | bytes 3145732
  7.2 104.8 %all-gather.2.cloned.1.call-start = ((), (), s32[]{:S(2)}) async-start(), calls=%async_computation.5 | async-start | bytes 7864320 | tf_op jit(solution)/shard_map/all_gather | solution.py:113
  7.2 3.2 %copy-start.6 = (s32[128,4]{0,1:T(4,128)S(1)}, s32[128,4]{0,1:T(4,128)}, u32[]{:S(2)}) copy-start(s32[128,4]{0,1:T(4,128)} %param.19) | copy-start | bytes 6148
  66.5 121.5 %reduce-scatter.5.cloned.1.call-start = ((), (), s32[]{:S(2)}) async-start(), calls=%async_computation.6 | async-start | bytes 7864320 | tf_op jit(solution)/shard_map/reduce_scatter | solution.py:121
  129.9 0.8 copy-start.3
  129.9 4.2 %copy-start.4 = (bf16[256,128]{1,0:T(8,128)(2,1)S(1)}, bf16[256,128]{1,0:T(8,128)(2,1)}, u32[]{:S(2)}) copy-start(bf16[256,128]{1,0:T(8,128)(2,1)} %param.14) | copy-start | bytes 196612
  129.9 8.5 %copy-start.5 = (bf16[256,512]{1,0:T(8,128)(2,1)S(1)}, bf16[256,512]{1,0:T(8,128)(2,1)}, u32[]{:S(2)}) copy-start(bf16[256,512]{1,0:T(8,128)(2,1)} %param.12) | copy-start | bytes 786436
  129.9 8.9 %copy-start.8 = (f32[8]{0:T(128)S(1)}, f32[8]{0:T(128)}, u32[]{:S(2)}) copy-start(f32[8]{0:T(128)} %param.15) | copy-start | bytes 100
  130.0 109.7 %reduce-scatter.3.cloned.1.call-start = ((), (), s32[]{:S(2)}) async-start(), calls=%async_computation.4 | async-start | bytes 2621440 | tf_op jit(solution)/shard_map/reduce_scatter | solution.py:83
  130.8 8.2 %collective-permute-start.1 = (bf16[128,128]{1,0:T(8,128)(2,1)S(1)}, bf16[128,128]{1,0:T(8,128)(2,1)S(1)}, u32[]{:S(2)}, u32[]{:S(2)}) collective-permute-start(bf16[128,128]{1,0:T(8,128)(2,1)S(1)} %slice.20), channel_id=1, source_target_pairs={{0,4},{4,8},{8,12},{12,16},{16,20},{20,24},{24,28},{1,5},{5,9},{9,... | collective-permute-start | bytes 98312 | tf_op jit(solution)/shard_map/ppermute | solution.py:18
  134.2 5.1 %collective-permute-start = (bf16[128,128]{1,0:T(8,128)(2,1)S(1)}, bf16[128,128]{1,0:T(8,128)(2,1)S(1)}, u32[]{:S(2)}, u32[]{:S(2)}) collective-permute-start(bf16[128,128]{1,0:T(8,128)(2,1)S(1)} %slice.18), channel_id=1, source_target_pairs={{0,4},{4,8},{8,12},{12,16},{16,20},{20,24},{24,28},{1,5},{5,9},{9,... | collective-permute-start | bytes 98312 | tf_op jit(solution)/shard_map/ppermute | solution.py:18
  140.5 2.5 %copy-start.2 = (bf16[512,4096]{1,0:T(8,128)(2,1)S(1)}, bf16[512,4096]{1,0:T(8,128)(2,1)}, u32[]{:S(2)}) copy-start(bf16[512,4096]{1,0:T(8,128)(2,1)} %param.16) | copy-start | bytes 12582916
  145.7 48.2 %copy-start.7 = (f32[128,4]{0,1:T(4,128)S(1)}, f32[128,4]{0,1:T(4,128)}, u32[]{:S(2)}) copy-start(f32[128,4]{0,1:T(4,128)} %param.20) | copy-start | bytes 6148
  188.0 42.4 %all-to-all-start.1 = ((bf16[8,96,1024]{2,1,0:T(8,128)(2,1)}), bf16[8,96,1024]{2,1,0:T(8,128)(2,1)}, u32[]{:S(2)}, u32[]{:S(2)}) async-start(bf16[8,96,1024]{2,1,0:T(8,128)(2,1)} %bitcast.63), calls=%async_computation.3 | async-start | bytes 3145728 | tf_op jit(solution)/shard_map/all_to_all | solution.py:124
Sparse Core Ops, SparseCore 0:
  66.6 45.3 all-gather.1
  130.1 57.8 reduce-scatter.4
  191.1 31.1 reduce-scatter.2
where the time goes:
time: 247 us; the launch traced here: 246 us
  waiting for transfers between devices  124 us (50%)
  blocking collectives  44.2 us (18%)
  matrix products  21.6 us (9%)
  local copies, waits for them, and re-layouts  17.5 us (7%)
  between operations  14.1 us (6%)
  starting transfers between devices  12.6 us (5%)
  other arithmetic  11.9 us (5%)
    all_gather x1, waiting for transfers between devices, shards(): portion = lax.all_gather(arrived, 'tp', axis=1, tiled=True)  45.5 us
    all_to_all x1, blocking collectives, shards(): lax.all_to_all(outgoing, 'ep', split_axis=0, concat_axis=0, tiled=True)  44.2 us
    reduce_scatter x1, waiting for transfers between devices, shards(): lax.psum_scatter(partial_value.astype(jnp.bfloat16), 'tp', scatter_dimens...  42.3 us
    all_to_all x1, waiting for transfers between devices, shards(): lax.all_to_all(expert_result.reshape(experts, capacity, col_share), 'ep',...  36.5 us
    dot_general x1, matrix products, shards(): jnp.dot(activated, down_weight[0], preferred_element_type=jnp.float32)  12.7 us
    ppermute x2, starting transfers between devices, passed_along(): return lax.ppermute(block, axis, route)  6.93 us
    gather x2, local copies, waits for them, and re-layouts, shards(): jnp.take(returned.reshape(experts * capacity, col_share), target, axis=0)  5.57 us
    all_to_all x1, starting transfers between devices, shards(): lax.all_to_all(expert_result.reshape(experts, capacity, col_share), 'ep',...  5.51 us
  transfers between devices with their start and end apart: 6, of which 3 were waited for; matrix products, arithmetic and copies ran while one was open for 6% of the time, Pallas kernels for 0%

commit v1 on v0

--- a/solution.py
+++ b/solution.py
@@ -110,7 +110,11 @@
     arrived = lax.all_to_all(outgoing, "ep", split_axis=0, concat_axis=0, tiled=True).reshape(
         experts * capacity, col_share
     )
-    portion = lax.all_gather(arrived, "tp", axis=1, tiled=True)
+    carry_the_spots = lambda buf: jnp.concatenate(
+        lax.all_to_all(jnp.stack([buf for _ in range(lax.psum(1, "tp"))], axis=0), "tp", 0, 0),
+        axis=1,
+    )
+    portion = carry_the_spots(arrived)
     gate_pre = jnp.dot(portion, gate_one, preferred_element_type=jnp.float32)
     up_pre = jnp.dot(portion, up_one, preferred_element_type=jnp.float32)
     gate_cut = jnp.minimum(gate_pre, CLAMP)

time: 247 us -> 277 us (1.12)
  blocking collectives: 44.2 us -> 118 us
  waiting for transfers between devices: 124 us -> 77.4 us
  local copies, waits for them, and re-layouts: 17.5 us -> 24.5 us
  matrix products: 21.6 us -> 18.2 us
    all_to_all x0 -> x1, blocking collectives: none -> 73.4 us  [shards(): lax.all_to_all(jnp.stack([buf for _ in range(lax.psum(1, 'tp'))], axis=0)...]
    all_gather x1 -> x0, waiting for transfers between devices: 45.5 us -> none  [shards(): portion = lax.all_gather(arrived, 'tp', axis=1, tiled=True)]
    another operation x1 -> x3, local copies, waits for them, and re-layouts: 0.01 us -> 4.41 us  [the longest x2 4.4 us: shards(): jnp.stack([buf for _ in range(lax.psum(1, 'tp'))], axis=0)]
    dot_general x1, matrix products: 5.2 us -> 1.82 us  [shards(): gate_pre = jnp.dot(portion, gate_one, preferred_element_type=jnp.float32)]
  transfers between devices with their start and end apart: 6 -> 5, of which waited for: 3 -> 2; matrix products, arithmetic and copies ran while one was open for 6% -> 6% of each run, Pallas kernels for 0% -> 0%
where the time goes in v1:
time: 277 us; the launch traced here: 276 us
  blocking collectives  118 us (43%)
  waiting for transfers between devices  77.4 us (28%)
  local copies, waits for them, and re-layouts  24.5 us (9%)
  matrix products  18.2 us (7%)
  between operations  14.4 us (5%)
  starting transfers between devices  12.1 us (4%)
  other arithmetic  11.9 us (4%)
    all_to_all x1, blocking collectives, shards(): lax.all_to_all(jnp.stack([buf for _ in range(lax.psum(1, 'tp'))], axis=0)...  73.4 us
    all_to_all x1, blocking collectives, shards(): lax.all_to_all(outgoing, 'ep', split_axis=0, concat_axis=0, tiled=True)  44.2 us
    reduce_scatter x1, waiting for transfers between devices, shards(): lax.psum_scatter(partial_value.astype(jnp.bfloat16), 'tp', scatter_dimens...  40.9 us
    all_to_all x1, waiting for transfers between devices, shards(): lax.all_to_all(expert_result.reshape(experts, capacity, col_share), 'ep',...  36.5 us
    dot_general x1, matrix products, shards(): jnp.dot(activated, down_weight[0], preferred_element_type=jnp.float32)  12.7 us
    ppermute x2, starting transfers between devices, passed_along(): return lax.ppermute(block, axis, route)  6.51 us
    gather x2, local copies, waits for them, and re-layouts, shards(): jnp.take(returned.reshape(experts * capacity, col_share), target, axis=0)  5.57 us
  transfers between devices with their start and end apart: 5, of which 2 were waited for; matrix products, arithmetic and copies ran while one was open for 6% of the time, Pallas kernels for 0%

profile of v1, /device:TPU:0, one launch (start us, length us, event | category | flops | bytes accessed | tf_op | source)
XLA Modules:
  0.0 276.1 jit_solution(7691838810430235147)
XLA Ops:
  7.2 2.9 %convert_element_type.41 = f32[128,4096]{1,0:T(8,128)} convert(bf16[128,4096]{1,0:T(8,128)(2,1)} %param.17) | non-fusion elementwise | flops 524288 | bytes 3145728 | tf_op jit(solution)/shard_map/convert_element_type | solution.py:93
  10.2 0.3 multiply_reduce_fusion.1
  10.8 1.1 reduce-window.6
  12.0 0.2 slice_reduce_fusion
  12.6 2.4 scatter_custom_fusion
  15.2 0.7 dynamic-slice
  15.9 1.1 fusion.33
  17.1 3.6 %gather_fusion = bf16[768,1024]{1,0:T(8,128)(2,1)} fusion(bf16[129,1024]{1,0:T(8,128)(2,1)S(1)} %concatenate.19, s32[1024]{0:T(1024)S(1)} %pad_clamp_fusion.1), kind=kCustom, calls=%fused_computation | custom fusion | bytes 3148800 | tf_op jit(solution)/shard_map/jit(_take)/gather | solution.py:109
  20.6 1.6 broadcast_select_fusion
  22.3 44.2 %all_to_all.15 = bf16[8,96,1024]{2,1,0:T(8,128)(2,1)} all-to-all(bf16[8,96,1024]{2,1,0:T(8,128)(2,1)S(1)} %broadcast_select_fusion), channel_id=1, replica_groups=mesh['ep'=8,'tp'=4] {'ep'}, dimensions={0} | all-to-all | bytes 3145728 | tf_op jit(solution)/shard_map/all_to_all | solution.py:110
  66.4 2.6 copy.52
  69.0 1.8 stack.3
  70.9 73.4 %all_to_all.16 = bf16[4,768,1024]{1,2,0:T(8,128)(2,1)S(1)} all-to-all(bf16[4,768,1024]{1,2,0:T(8,128)(2,1)S(1)} %stack.3), channel_id=1, replica_groups=mesh['ep'=8,'tp'=4] {'tp'}, dimensions={0} | all-to-all | bytes 12582912 | tf_op jit(solution)/shard_map/all_to_all | solution.py:114
  144.3 2.7 copy-done.1
  146.9 1.8 fusion.9
  148.8 12.7 %convolution_convert_fusion = bf16[768,4096]{1,0:T(8,128)(2,1)} fusion(bf16[1,256,4096]{2,1,0:T(8,128)(2,1)S(1)} %copy-done, f32[768,256]{1,0:T(8,128)S(1)} %fusion.9, bf16[768,4096]{0,1:T(8,128)(2,1)} %bitcast.65, bf16[1,4096,256]{2,1,0:T(8,128)(2,1)} %param.22), kind=kOutput, calls=%fused_computation.3 | convolution fusion | flops 3226140672 | bytes 17563648 | tf_op jit(solution)/shard_map/dot_general | solution.py:124
  161.5 0.8 copy-done.5
  162.3 3.3 %collective-permute-start.1 = (bf16[128,128]{1,0:T(8,128)(2,1)S(1)}, bf16[128,128]{1,0:T(8,128)(2,1)S(1)}, u32[]{:S(2)}, u32[]{:S(2)}) collective-permute-start(bf16[128,128]{1,0:T(8,128)(2,1)S(1)} %slice.20), channel_id=1, source_target_pairs={{0,4},{4,8},{8,12},{12,16},{16,20},{20,24},{24,28},{1,5},{5,9},{9,... | collective-permute-start | bytes 98312 | tf_op jit(solution)/shard_map/ppermute | solution.py:18
  165.6 3.2 %collective-permute-start = (bf16[128,128]{1,0:T(8,128)(2,1)S(1)}, bf16[128,128]{1,0:T(8,128)(2,1)S(1)}, u32[]{:S(2)}, u32[]{:S(2)}) collective-permute-start(bf16[128,128]{1,0:T(8,128)(2,1)S(1)} %slice.18), channel_id=1, source_target_pairs={{0,4},{4,8},{8,12},{12,16},{16,20},{20,24},{24,28},{1,5},{5,9},{9,... | collective-permute-start | bytes 98312 | tf_op jit(solution)/shard_map/ppermute | solution.py:18
  169.5 0.3 reshape.261
  170.6 0.5 fusion.60
  171.2 0.3 fusion.5
  171.6 0.5 fusion.26
  172.1 0.3 copy.46
  172.4 1.6 copy-done.3
  174.0 2.7 convolution_convert_fusion.1
  176.7 40.9 %reduce-scatter.5.cloned.1.call-done = bf16[768,1024]{1,0:T(8,128)(2,1)} async-done(((bf16[768,4096]{1,0:T(8,128)(2,1)}), bf16[768,1024]{1,0:T(8,128)(2,1)}) %reduce-scatter.5.cloned.1.call-update) | async-done | bytes 1572880 | tf_op jit(solution)/shard_map/reduce_scatter | solution.py:125
  217.6 5.5 %all-to-all-start.2 = ((bf16[8,96,1024]{2,1,0:T(8,128)(2,1)}), bf16[8,96,1024]{2,1,0:T(8,128)(2,1)}, u32[]{:S(2)}, u32[]{:S(2)}) async-start(bf16[8,96,1024]{2,1,0:T(8,128)(2,1)} %bitcast.68), calls=%async_computation.4 | async-start | bytes 3145728 | tf_op jit(solution)/shard_map/all_to_all | solution.py:128
  223.6 36.5 %all-to-all-done.2 = bf16[8,96,1024]{2,1,0:T(8,128)(2,1)} async-done(((bf16[8,96,1024]{2,1,0:T(8,128)(2,1)}), bf16[8,96,1024]{2,1,0:T(8,128)(2,1)}, u32[]{:S(2)}, u32[]{:S(2)}) %all-to-all-start.2) | async-done | bytes 1572896 | tf_op jit(solution)/shard_map/all_to_all | solution.py:128
  260.1 4.3 %gather_fusion.1 = bf16[512,1024]{1,0:T(8,128)(2,1)S(1)} fusion(bf16[768,1024]{1,0:T(8,128)(2,1)} %bitcast.19, s32[1024]{0:T(1024)S(1)} %pad_clamp_fusion), kind=kCustom, calls=%fused_computation.1 | custom fusion | bytes 2099200 | tf_op jit(solution)/shard_map/jit(_take)/gather | solution.py:135
  264.4 1.2 gather.15
  265.6 3.6 %multiply_reduce_fusion = bf16[128,1024]{1,0:T(8,128)(2,1)} fusion(f32[128,4]{1,0:T(8,128)S(1)} %copy.53, bf16[128,4,1024]{2,1,0:T(4,128)(2,1)} %gather.15, pred[128,4]{1,0:T(8,128)(4,1)S(1)} %copy.50), kind=kLoop, calls=%fused_computation.11 | loop fusion | flops 1966080 | bytes 1313280 | tf_op jit(solution)/shard_map/reduce_sum | solution.py:137
  (70 shorter events, 2.9 us)
Async XLA Ops:
  7.2 141.6 %copy-start = (bf16[1,256,4096]{2,1,0:T(8,128)(2,1)S(1)}, bf16[1,256,4096]{2,1,0:T(8,128)(2,1)}, u32[]{:S(2)}) copy-start(bf16[1,256,4096]{2,1,0:T(8,128)(2,1)} %param.23) | copy-start | bytes 6291460
  7.2 3.0 %copy-start.2 = (bf16[128,4096]{1,0:T(8,128)(2,1)S(1)}, bf16[128,4096]{1,0:T(8,128)(2,1)}, u32[]{:S(2)}) copy-start(bf16[128,4096]{1,0:T(8,128)(2,1)} %param.17) | copy-start | bytes 3145732
  7.2 210.4 %reduce-scatter.5.cloned.1.call-start = ((), (), s32[]{:S(2)}) async-start(), calls=%async_computation.6 | async-start | bytes 7864320 | tf_op jit(solution)/shard_map/reduce_scatter | solution.py:125
  7.2 3.2 %copy-start.8 = (s32[128,4]{0,1:T(4,128)S(1)}, s32[128,4]{0,1:T(4,128)}, u32[]{:S(2)}) copy-start(s32[128,4]{0,1:T(4,128)} %param.19) | copy-start | bytes 6148
  70.9 76.1 %copy-start.4 = (bf16[1,4096,256]{2,1,0:T(8,128)(2,1)S(1)}, bf16[1,4096,256]{2,1,0:T(8,128)(2,1)}, u32[]{:S(2)}) copy-start(bf16[1,4096,256]{2,1,0:T(8,128)(2,1)} %param.21) | copy-start | bytes 6291460
  144.3 2.7 copy-start.1
  161.4 0.8 copy-start.5
  161.4 4.2 %copy-start.6 = (bf16[256,128]{1,0:T(8,128)(2,1)S(1)}, bf16[256,128]{1,0:T(8,128)(2,1)}, u32[]{:S(2)}) copy-start(bf16[256,128]{1,0:T(8,128)(2,1)} %param.14) | copy-start | bytes 196612
  161.5 8.1 %copy-start.7 = (bf16[256,512]{1,0:T(8,128)(2,1)S(1)}, bf16[256,512]{1,0:T(8,128)(2,1)}, u32[]{:S(2)}) copy-start(bf16[256,512]{1,0:T(8,128)(2,1)} %param.12) | copy-start | bytes 786436
  161.5 8.4 %copy-start.10 = (f32[8]{0:T(128)S(1)}, f32[8]{0:T(128)}, u32[]{:S(2)}) copy-start(f32[8]{0:T(128)} %param.15) | copy-start | bytes 100
  161.5 107.8 %reduce-scatter.3.cloned.1.call-start = ((), (), s32[]{:S(2)}) async-start(), calls=%async_computation.5 | async-start | bytes 2621440 | tf_op jit(solution)/shard_map/reduce_scatter | solution.py:83
  162.3 7.8 %collective-permute-start.1 = (bf16[128,128]{1,0:T(8,128)(2,1)S(1)}, bf16[128,128]{1,0:T(8,128)(2,1)S(1)}, u32[]{:S(2)}, u32[]{:S(2)}) collective-permute-start(bf16[128,128]{1,0:T(8,128)(2,1)S(1)} %slice.20), channel_id=1, source_target_pairs={{0,4},{4,8},{8,12},{12,16},{16,20},{20,24},{24,28},{1,5},{5,9},{9,... | collective-permute-start | bytes 98312 | tf_op jit(solution)/shard_map/ppermute | solution.py:18
  165.6 4.7 %collective-permute-start = (bf16[128,128]{1,0:T(8,128)(2,1)S(1)}, bf16[128,128]{1,0:T(8,128)(2,1)S(1)}, u32[]{:S(2)}, u32[]{:S(2)}) collective-permute-start(bf16[128,128]{1,0:T(8,128)(2,1)S(1)} %slice.18), channel_id=1, source_target_pairs={{0,4},{4,8},{8,12},{12,16},{16,20},{20,24},{24,28},{1,5},{5,9},{9,... | collective-permute-start | bytes 98312 | tf_op jit(solution)/shard_map/ppermute | solution.py:18
  171.6 2.4 copy-start.3
  176.7 46.8 %copy-start.9 = (f32[128,4]{0,1:T(4,128)S(1)}, f32[128,4]{0,1:T(4,128)}, u32[]{:S(2)}) copy-start(f32[128,4]{0,1:T(4,128)} %param.20) | copy-start | bytes 6148
  217.6 42.4 %all-to-all-start.2 = ((bf16[8,96,1024]{2,1,0:T(8,128)(2,1)}), bf16[8,96,1024]{2,1,0:T(8,128)(2,1)}, u32[]{:S(2)}, u32[]{:S(2)}) async-start(bf16[8,96,1024]{2,1,0:T(8,128)(2,1)} %bitcast.68), calls=%async_computation.4 | async-start | bytes 3145728 | tf_op jit(solution)/shard_map/all_to_all | solution.py:128
Sparse Core Ops, SparseCore 0:
  161.6 55.9 reduce-scatter.4
  220.7 31.1 reduce-scatter.2
